TPU v7x, 512 devices: a whole 4x8x8 slice. The times are simulated.
512 devices in a mesh: gr: 2 (over z_hi), fs: 32 (over z_lo, y), tp: 8 (over x, core).
Axes of the slice: x: 4, y: 8, z: 8 (z_hi: 2, z_lo: 4; z = z_hi * 4 + z_lo), core: 2. Of those that a mesh axis runs over, the one named last changes fastest.
Arguments:
- prompt: bfloat16 [16, 256, 2048], P(('gr', 'tp')), as said below
- norm_gain: float32 [2, 2048], P(None, 'fs'), may hold values from 0.1 to 1.9
- gate_weight: float32 [2, 2048, 4096], P(None, 'fs', ('gr', 'tp')), may hold values from -0.125 to 0.125
- up_weight: float32 [2, 2048, 4096], P(None, 'fs', ('gr', 'tp')), may hold values from -0.125 to 0.125
- down_weight: float32 [2, 4096, 2048], P(None, 'fs', ('gr', 'tp')), may hold values from -0.09375 to 0.09375
Outputs:
- gate_sampler: bfloat16 [2, 2048, 4096], P(None, None, 'fs')
- up_sampler: bfloat16 [2, 2048, 4096], P(None, None, 'fs')
- down_sampler: bfloat16 [2, 4096, 2048], P(None, 'fs')
- mixed: bfloat16 [16, 256, 2048], P(('gr', 'tp'))
Inputs may be any that keep to these rules, and one draw needn't show every extreme that they name: prompt features have scales that differ from feature to feature.
All inputs are finite; a program needn't handle non-finite values.
Results may differ from a plain program's by a relative error of at most 0.0043.
Values may be sent and summed in bfloat16 or wider, within the bound.
No kernel may reach another device: no remote copies, remote signals or barrier semaphores. Data moves between devices by JAX's collectives and lax.ppermute only.
A program may use at most 64 MiB of HBM per device.

v0:
```python
import jax
import jax.numpy as jnp
from jax import lax
from jax.experimental import pallas as pl
from jax.experimental.pallas import tpu as pltpu
from jax.sharding import Mesh
from jax.sharding import PartitionSpec as P


norm_eps = 1e-06
bf16 = jnp.bfloat16
f32 = jnp.float32

AXES = ("gr", "zl", "yh", "yl", "x", "core")
SIZES = (2, 4, 4, 2, 4, 2)
FS = ("zl", "yh", "yl")
GT = ("gr", "x", "core")
SWAP = [(0, 1), (1, 0)]


def device(gr, fs, tp):
    return gr * 256 + fs * 8 + tp


def everyone():
    return [(gr, fs, tp) for gr in range(2) for fs in range(32) for tp in range(8)]


def weight_moves():
    moves = []
    for gr, fs, tp in everyone():
        to = device(fs >> 4, 2 * (8 * gr + tp) + (fs & 1), (fs >> 1) & 7)
        moves.append((device(gr, fs, tp), to))
    return moves


def in_vmem(value):
    return pltpu.with_memory_space_constraint(value, pltpu.VMEM)


def kernel(body, outs, scratch=()):
    here = pl.BlockSpec(memory_space=pltpu.VMEM)

    def call(*args):
        return pl.pallas_call(
            body,
            in_specs=[here] * len(args),
            out_specs=tuple(here for _ in outs),
            out_shape=tuple(pltpu.VMEM(shape, bf16) for shape in outs),
            scratch_shapes=[pltpu.VMEM(shape, bf16) for shape in scratch],
            compiler_params=pltpu.CompilerParams(vmem_limit_bytes=24 << 20),
        )(*[in_vmem(a) for a in args])

    return call


def in_order(first, second, swapped):
    return jnp.where(swapped, second, first), jnp.where(swapped, first, second)


def to_everyone(value, axes, count):
    return lax.all_to_all(
        jnp.broadcast_to(value[None], (count, *value.shape)), axes, 0, 0, tiled=True
    )


def layer_call(late, normed, own, other):
    def body(normed, own, other, gate, up, served, part, wide, down):
        core = lax.axis_index("core") == 0
        even = lax.axis_index("yl") == 0
        for k in range(4):
            x = lax.axis_index("x") ^ k if late else k
            for b in range(2):
                for s in range(3):
                    mn = own[k, b, 128 * s : 128 * s + 128]
                    ot = other[k, b, 128 * s : 128 * s + 128]
                    for c in range(2):
                        line = jnp.where(core, mn, ot) if c == 0 else jnp.where(core, ot, mn)
                        at = 128 * c + 64 * b
                        if s < 2:
                            wide[s, x, at : at + 64, :256] = line[:64]
                            wide[s, x, at : at + 64, 256:] = line[64:]
                        else:
                            for g in range(2):
                                down[g, x, 128 * b : 128 * b + 128, 128 * c : 128 * c + 128] = line[
                                    :, 128 * g : 128 * g + 128
                                ]
        act = jnp.zeros((128, 512), f32)
        for s in range(2):
            for x in range(4):
                at = 1024 * s + 256 * x
                block = wide[s, x]
                gate[at : at + 256] = jnp.where(even, block[:, :128], block[:, 128:256])
                up[at : at + 256] = jnp.where(even, block[:, 256:384], block[:, 384:])
                act = act + jnp.dot(normed[:, at : at + 256], block, preferred_element_type=f32)
        gate_act, up_act = act[:, :256], act[:, 256:]
        hidden = (gate_act / (1.0 + jnp.exp(-gate_act)) * up_act).astype(bf16)
        for g in range(2):
            for x in range(4):
                at = 1024 * g + 256 * x
                block = down[g, x]
                served[:, at : at + 256] = jnp.where(even, block[:128], block[128:])
                out = jnp.dot(hidden, block, preferred_element_type=f32)
                part[:, at : at + 256] = out.astype(bf16)

    outs = ((2048, 128), (2048, 128), (128, 2048), (128, 2048))
    scratch = ((2, 4, 256, 512), (2, 4, 256, 256))
    return kernel(body, outs, scratch)(normed, own, other)


def normalised(value):
    mean = jnp.sum(value * value, axis=1, keepdims=True) * (1.0 / 2048)
    return (value * lax.rsqrt(mean + norm_eps)).astype(bf16)


def norm_call(stream):
    def body(stream, out):
        out[...] = normalised(stream[...].astype(f32))

    return kernel(body, (stream.shape,))(stream)[0]


def step(prompt, norm_gain, gate_weight, up_weight, down_weight):
    gain = norm_gain[:, :, None]
    gate = (gain * gate_weight).astype(bf16)
    up = (gain * up_weight).astype(bf16)
    high = lax.axis_index("gr") == 1
    moved = []
    for layer in range(2):
        block = jnp.concatenate([gate[layer], up[layer]], axis=0)
        moved.append(lax.ppermute(block, AXES, weight_moves()))
    down = down_weight.astype(bf16)
    both = jnp.concatenate([moved[0], jnp.concatenate([down[0], down[1]], axis=1)], axis=0)
    across = lax.ppermute(both, "gr", SWAP)
    low, top = in_order(both, across, high)

    def downs(layer):
        cols = slice(128 * layer, 128 * layer + 128)
        return jnp.concatenate([low[128:, cols], top[128:, cols]], axis=1)

    block = jnp.concatenate([low[:128], top[:128], downs(0)], axis=0)
    own = to_everyone(block, ("x", "yl"), 8)
    across = lax.ppermute(moved[1], "gr", SWAP)
    block = jnp.concatenate([*in_order(moved[1], across, high), downs(1)], axis=0)
    yl = lax.axis_index("yl")
    came = lax.ppermute(block, "yl", SWAP)
    own, block = lax.optimization_barrier((own, block))
    other = lax.ppermute(own, "core", SWAP)
    pair = jnp.stack(in_order(block, came, yl == 1))
    late = [lax.ppermute(pair, "x", [(x, x ^ k) for x in range(4)]) for k in (1, 2, 3)]
    late = jnp.stack([pair, *late])
    late_other = lax.ppermute(late, "core", SWAP)

    half = lax.dynamic_slice_in_dim(prompt[0], yl * 128, 128, 0)
    mine = lax.dynamic_slice_in_dim(half, lax.axis_index(("zl", "yh")) * 8, 8, 0).astype(f32)
    normed = norm_call(half)
    early = [a.reshape(4, 2, 384, 256) for a in (own, other)]
    gates, ups, served = [], [], []
    for layer in range(2):
        pieces = (late, late_other) if layer else early
        gate, up, down, part = layer_call(layer == 1, normed, *pieces)
        gates.append(gate)
        ups.append(up)
        served.append(down)
        parts = lax.all_to_all(part.reshape(16, 8, 2048), ("zl", "yh"), 0, 0, tiled=True)
        mine = mine + 0.5 * jnp.sum(parts.astype(f32), axis=0)
        if layer == 0:
            normed = to_everyone(normalised(mine), ("zl", "yh"), 16).reshape(128, 2048)
        else:
            mixed = to_everyone(mine.astype(bf16), ("yl", "zl", "yh"), 32)
    return jnp.stack(gates), jnp.stack(ups), jnp.stack(served), mixed.reshape(prompt.shape)


def solution(mesh):
    fine = Mesh(mesh.devices.reshape(SIZES), AXES)
    in_specs = (P(GT, None, None), P(None, FS), P(None, FS, GT), P(None, FS, GT), P(None, FS, GT))
    out_specs = (P(None, None, FS), P(None, None, FS), P(None, FS, None), P(GT, None, None))
    return jax.shard_map(step, mesh=fine, in_specs=in_specs, out_specs=out_specs, check_vma=False)
```

profile of v0, /device:TPU:22, one launch (start us, length us, event | category | flops | bytes accessed | tf_op | source)
XLA Modules:
  0.0 215.4 jit_solution(16851037060433546591)
XLA Ops:
  0.6 1.1 multiply_convert_fusion.1
  1.7 6.9 %collective-permute-start = (bf16[128,256]{1,0:T(8,128)(2,1)S(1)}, bf16[128,256]{1,0:T(8,128)(2,1)S(1)}, u32[]{:S(2)}, u32[]{:S(2)}) collective-permute-start(bf16[128,256]{1,0:T(8,128)(2,1)S(1)} %pad_maximum_fusion.5), channel_id=1, source_target_pairs={{0,0},{1,16},{2,32},{3,48},{4,64},{5,80},{6,96},{7,112},{8,8},{9,2... | collective-permute-start | bytes 196616 | tf_op jit(solution)/shard_map/ppermute | solution.py:131
  9.6 2.9 %collective-permute-done = bf16[128,256]{1,0:T(8,128)(2,1)S(1)} collective-permute-done((bf16[128,256]{1,0:T(8,128)(2,1)S(1)}, bf16[128,256]{1,0:T(8,128)(2,1)S(1)}, u32[]{:S(2)}, u32[]{:S(2)}) %collective-permute-start) | collective-permute-done | bytes 65568 | tf_op jit(solution)/shard_map/ppermute | solution.py:131
  12.5 13.3 %collective-permute-start.1 = (bf16[256,256]{1,0:T(8,128)(2,1)S(1)}, bf16[256,256]{1,0:T(8,128)(2,1)S(1)}, u32[]{:S(2)}, u32[]{:S(2)}) collective-permute-start(bf16[256,256]{1,0:T(8,128)(2,1)S(1)} %maximum_maximum_fusion.2), channel_id=1, source_target_pairs={{0,256},{256,0},{1,257},{257,1},{2,258},{258,2},{3,259},{259,3},{4... | collective-permute-start | bytes 393224 | tf_op jit(solution)/shard_map/ppermute | solution.py:134
  25.7 3.8 %collective-permute-done.1 = bf16[256,256]{1,0:T(8,128)(2,1)S(1)} collective-permute-done((bf16[256,256]{1,0:T(8,128)(2,1)S(1)}, bf16[256,256]{1,0:T(8,128)(2,1)S(1)}, u32[]{:S(2)}, u32[]{:S(2)}) %collective-permute-start.1) | collective-permute-done | bytes 131104 | tf_op jit(solution)/shard_map/ppermute | solution.py:134
  29.7 1.3 broadcast_in_dim.10
  31.0 6.8 %all-to-all-start = ((bf16[8,384,256]{2,1,0:T(8,128)(2,1)}), bf16[8,384,256]{2,1,0:T(8,128)(2,1)S(1)}, u32[]{:S(2)}, u32[]{:S(2)}) async-start(bf16[8,384,256]{2,1,0:T(8,128)(2,1)} %broadcast_in_dim.10), calls=%async_computation | async-start | bytes 3145728 | tf_op jit(solution)/shard_map/all_to_all | solution.py:62
  37.8 5.4 %collective-permute-start.2 = (bf16[128,256]{1,0:T(8,128)(2,1)S(1)}, bf16[128,256]{1,0:T(8,128)(2,1)S(1)}, u32[]{:S(2)}, u32[]{:S(2)}) collective-permute-start(bf16[128,256]{1,0:T(8,128)(2,1)S(1)} %pad_maximum_fusion.6), channel_id=1, source_target_pairs={{0,0},{1,16},{2,32},{3,48},{4,64},{5,80},{6,96},{7,112},{8,8},{9,2... | collective-permute-start | bytes 196616 | tf_op jit(solution)/shard_map/ppermute | solution.py:131
  43.2 15.7 %collective-permute-done.2 = bf16[128,256]{1,0:T(8,128)(2,1)S(1)} collective-permute-done((bf16[128,256]{1,0:T(8,128)(2,1)S(1)}, bf16[128,256]{1,0:T(8,128)(2,1)S(1)}, u32[]{:S(2)}, u32[]{:S(2)}) %collective-permute-start.2) | collective-permute-done | bytes 65568 | tf_op jit(solution)/shard_map/ppermute | solution.py:131
  58.9 7.4 %collective-permute-start.3 = (bf16[128,256]{1,0:T(8,128)(2,1)S(1)}, bf16[128,256]{1,0:T(8,128)(2,1)S(1)}, u32[]{:S(2)}, u32[]{:S(2)}) collective-permute-start(bf16[128,256]{1,0:T(8,128)(2,1)S(1)} %collective-permute-done.2), channel_id=1, source_target_pairs={{0,256},{256,0},{1,257},{257,1},{2,258},{258,2},{3,259},{259,3},{4... | collective-permute-start | bytes 196616 | tf_op jit(solution)/shard_map/ppermute | solution.py:143
  66.3 2.6 %collective-permute-done.3 = bf16[128,256]{1,0:T(8,128)(2,1)S(1)} collective-permute-done((bf16[128,256]{1,0:T(8,128)(2,1)S(1)}, bf16[128,256]{1,0:T(8,128)(2,1)S(1)}, u32[]{:S(2)}, u32[]{:S(2)}) %collective-permute-start.3) | collective-permute-done | bytes 65568 | tf_op jit(solution)/shard_map/ppermute | solution.py:143
  69.0 6.0 %collective-permute-start.4 = (bf16[8,384,256]{2,1,0:T(8,128)(2,1)S(1)}, bf16[8,384,256]{2,1,0:T(8,128)(2,1)S(1)}, u32[]{:S(2)}, u32[]{:S(2)}) collective-permute-start(bf16[8,384,256]{2,1,0:T(8,128)(2,1)S(1)} %all-to-all-done), channel_id=1, source_target_pairs={{0,1},{1,0},{2,3},{3,2},{4,5},{5,4},{6,7},{7,6},{8,9},{9,8},{10,11... | collective-permute-start | bytes 4718600 | tf_op jit(solution)/shard_map/ppermute | solution.py:148
  75.0 3.4 %collective-permute-start.5 = (bf16[384,256]{1,0:T(8,128)(2,1)S(1)}, bf16[384,256]{1,0:T(8,128)(2,1)S(1)}, u32[]{:S(2)}, u32[]{:S(2)}) collective-permute-start(bf16[384,256]{1,0:T(8,128)(2,1)S(1)} %maximum_maximum_fusion.1), channel_id=1, source_target_pairs={{0,8},{8,0},{1,9},{9,1},{2,10},{10,2},{3,11},{11,3},{4,12},{12,4},... | collective-permute-start | bytes 589832 | tf_op jit(solution)/shard_map/ppermute | solution.py:146
  78.5 1.1 dynamic-slice_bitcast_fusion.stream
  84.0 10.4 %all-to-all-start.1 = ((bf16[16,8,2048]{2,1,0:T(8,128)(2,1)}), bf16[16,8,2048]{2,1,0:T(8,128)(2,1)S(1)}, u32[]{:S(2)}, u32[]{:S(2)}) async-start(bf16[16,8,2048]{2,1,0:T(8,128)(2,1)} %bitcast.66), calls=%async_computation.1 | async-start | bytes 1048576 | tf_op jit(solution)/shard_map/all_to_all | solution.py:165
  94.5 1.9 collective-permute-start.8
  96.4 1.9 collective-permute-start.7
  98.3 6.0 %collective-permute-start.6 = (bf16[2,384,256]{2,1,0:T(8,128)(2,1)S(1)}, bf16[2,384,256]{2,1,0:T(8,128)(2,1)}, u32[]{:S(2)}, u32[]{:S(2)}) collective-permute-start(bf16[2,384,256]{2,1,0:T(8,128)(2,1)S(1)} %get-tuple-element.25), channel_id=1, source_target_pairs={{0,2},{2,0},{4,6},{6,4},{1,3},{3,1},{5,7},{7,5},{8,10},{10,8},{12,... | collective-permute-start | bytes 1179656 | tf_op jit(solution)/shard_map/ppermute | solution.py:150
  104.3 11.9 %collective-permute-done.8 = bf16[2,384,256]{2,1,0:T(8,128)(2,1)S(1)} collective-permute-done((bf16[2,384,256]{2,1,0:T(8,128)(2,1)S(1)}, bf16[2,384,256]{2,1,0:T(8,128)(2,1)S(1)}, u32[]{:S(2)}, u32[]{:S(2)}) %collective-permute-start.8) | collective-permute-done | bytes 393248 | tf_op jit(solution)/shard_map/ppermute | solution.py:150
  116.2 2.6 %collective-permute-done.6 = bf16[2,384,256]{2,1,0:T(8,128)(2,1)} collective-permute-done((bf16[2,384,256]{2,1,0:T(8,128)(2,1)S(1)}, bf16[2,384,256]{2,1,0:T(8,128)(2,1)}, u32[]{:S(2)}, u32[]{:S(2)}) %collective-permute-start.6) | collective-permute-done | bytes 393248 | tf_op jit(solution)/shard_map/ppermute | solution.py:150
  118.8 1.2 pad_maximum_fusion.own
  120.0 1.9 collective-permute-start.9
  124.8 9.9 %all-to-all-start.2 = ((bf16[16,8,2048]{2,1,0:T(8,128)(2,1)}), bf16[16,8,2048]{2,1,0:T(8,128)(2,1)S(1)}, u32[]{:S(2)}, u32[]{:S(2)}) async-start(bf16[16,8,2048]{2,1,0:T(8,128)(2,1)} %broadcast_in_dim.12), calls=%async_computation.2 | async-start | bytes 1048576 | tf_op jit(solution)/shard_map/all_to_all | solution.py:62
  134.7 18.0 %all-to-all-done.2 = bf16[16,8,2048]{2,1,0:T(8,128)(2,1)S(1)} async-done(((bf16[16,8,2048]{2,1,0:T(8,128)(2,1)}), bf16[16,8,2048]{2,1,0:T(8,128)(2,1)S(1)}, u32[]{:S(2)}, u32[]{:S(2)}) %all-to-all-start.2) | async-done | bytes 524320 | tf_op jit(solution)/shard_map/all_to_all | solution.py:62
  152.8 2.4 %shard_map.86 = (bf16[2048,128]{1,0:T(8,128)(2,1)S(1)}, bf16[2048,128]{1,0:T(8,128)(2,1)S(1)}, bf16[128,2048]{1,0:T(8,128)(2,1)S(1)}, bf16[128,2048]{1,0:T(8,128)(2,1)S(1)}) custom-call(bf16[128,2048]{1,0:T(8,128)(2,1)S(1)} %bitcast.64, bf16[4,2,384,256]{3,2,1,0:T(8,128)(2,1)S(1)} %pad_maximum_fusion.own, bf16[4,2,384,256]{3,2,1,0:T(8,128)(2,1)} %collective-permute-done.9.other), custom_call_target="tpu_custom_call" | custom-call | tf_op jit(solution)/shard_map/pallas_call | solution.py:45
  155.2 23.2 %all_to_all.25 = bf16[16,8,2048]{2,1,0:T(8,128)(2,1)S(1)} all-to-all(bf16[16,8,2048]{2,1,0:T(8,128)(2,1)S(1)} %bitcast.67), channel_id=1, replica_groups=mesh['gr'=2,'zl'=4,'yh'=4,'yl'=2,'x'=4,'core'=2] {'zl','yh'}, dimensions={0} | all-to-all | bytes 1048576 | tf_op jit(solution)/shard_map/all_to_all | solution.py:165
  179.4 1.1 broadcast_in_dim.28
  180.5 5.7 %all-to-all-start.4 = ((bf16[32,8,2048]{2,1,0:T(8,128)(2,1)}), bf16[32,8,2048]{2,1,0:T(8,128)(2,1)S(1)}, u32[]{:S(2)}, u32[]{:S(2)}) async-start(bf16[32,8,2048]{2,1,0:T(8,128)(2,1)} %broadcast_in_dim.28), calls=%async_computation.4 | async-start | bytes 2097152 | tf_op jit(solution)/shard_map/all_to_all | solution.py:62
  186.2 1.1 pad_maximum_fusion.1
  187.3 1.1 pad_maximum_fusion.2
  188.4 1.1 pad_maximum_fusion.3
  189.5 24.9 %all-to-all-done.4 = bf16[32,8,2048]{2,1,0:T(8,128)(2,1)S(1)} async-done(((bf16[32,8,2048]{2,1,0:T(8,128)(2,1)}), bf16[32,8,2048]{2,1,0:T(8,128)(2,1)S(1)}, u32[]{:S(2)}, u32[]{:S(2)}) %all-to-all-start.4) | async-done | bytes 1048608 | tf_op jit(solution)/shard_map/all_to_all | solution.py:62
  (50 shorter events, 10.4 us)
Async XLA Ops:
  1.7 10.7 %collective-permute-start = (bf16[128,256]{1,0:T(8,128)(2,1)S(1)}, bf16[128,256]{1,0:T(8,128)(2,1)S(1)}, u32[]{:S(2)}, u32[]{:S(2)}) collective-permute-start(bf16[128,256]{1,0:T(8,128)(2,1)S(1)} %pad_maximum_fusion.5), channel_id=1, source_target_pairs={{0,0},{1,16},{2,32},{3,48},{4,64},{5,80},{6,96},{7,112},{8,8},{9,2... | collective-permute-start | bytes 196616 | tf_op jit(solution)/shard_map/ppermute | solution.py:131
  12.5 17.1 %collective-permute-start.1 = (bf16[256,256]{1,0:T(8,128)(2,1)S(1)}, bf16[256,256]{1,0:T(8,128)(2,1)S(1)}, u32[]{:S(2)}, u32[]{:S(2)}) collective-permute-start(bf16[256,256]{1,0:T(8,128)(2,1)S(1)} %maximum_maximum_fusion.2), channel_id=1, source_target_pairs={{0,256},{256,0},{1,257},{257,1},{2,258},{258,2},{3,259},{259,3},{4... | collective-permute-start | bytes 393224 | tf_op jit(solution)/shard_map/ppermute | solution.py:134
  31.0 38.0 %all-to-all-start = ((bf16[8,384,256]{2,1,0:T(8,128)(2,1)}), bf16[8,384,256]{2,1,0:T(8,128)(2,1)S(1)}, u32[]{:S(2)}, u32[]{:S(2)}) async-start(bf16[8,384,256]{2,1,0:T(8,128)(2,1)} %broadcast_in_dim.10), calls=%async_computation | async-start | bytes 3145728 | tf_op jit(solution)/shard_map/all_to_all | solution.py:62
  37.8 21.1 %collective-permute-start.2 = (bf16[128,256]{1,0:T(8,128)(2,1)S(1)}, bf16[128,256]{1,0:T(8,128)(2,1)S(1)}, u32[]{:S(2)}, u32[]{:S(2)}) collective-permute-start(bf16[128,256]{1,0:T(8,128)(2,1)S(1)} %pad_maximum_fusion.6), channel_id=1, source_target_pairs={{0,0},{1,16},{2,32},{3,48},{4,64},{5,80},{6,96},{7,112},{8,8},{9,2... | collective-permute-start | bytes 196616 | tf_op jit(solution)/shard_map/ppermute | solution.py:131
  58.9 10.1 %collective-permute-start.3 = (bf16[128,256]{1,0:T(8,128)(2,1)S(1)}, bf16[128,256]{1,0:T(8,128)(2,1)S(1)}, u32[]{:S(2)}, u32[]{:S(2)}) collective-permute-start(bf16[128,256]{1,0:T(8,128)(2,1)S(1)} %collective-permute-done.2), channel_id=1, source_target_pairs={{0,256},{256,0},{1,257},{257,1},{2,258},{258,2},{3,259},{259,3},{4... | collective-permute-start | bytes 196616 | tf_op jit(solution)/shard_map/ppermute | solution.py:143
  69.0 10.7 %collective-permute-start.4 = (bf16[8,384,256]{2,1,0:T(8,128)(2,1)S(1)}, bf16[8,384,256]{2,1,0:T(8,128)(2,1)S(1)}, u32[]{:S(2)}, u32[]{:S(2)}) collective-permute-start(bf16[8,384,256]{2,1,0:T(8,128)(2,1)S(1)} %all-to-all-done), channel_id=1, source_target_pairs={{0,1},{1,0},{2,3},{3,2},{4,5},{5,4},{6,7},{7,6},{8,9},{9,8},{10,11... | collective-permute-start | bytes 4718600 | tf_op jit(solution)/shard_map/ppermute | solution.py:148
  75.0 19.3 %collective-permute-start.5 = (bf16[384,256]{1,0:T(8,128)(2,1)S(1)}, bf16[384,256]{1,0:T(8,128)(2,1)S(1)}, u32[]{:S(2)}, u32[]{:S(2)}) collective-permute-start(bf16[384,256]{1,0:T(8,128)(2,1)S(1)} %maximum_maximum_fusion.1), channel_id=1, source_target_pairs={{0,8},{8,0},{1,9},{9,1},{2,10},{10,2},{3,11},{11,3},{4,12},{12,4},... | collective-permute-start | bytes 589832 | tf_op jit(solution)/shard_map/ppermute | solution.py:146
  80.8 0.8 copy-start
  81.6 0.8 copy-start.1
  82.4 0.8 copy-start.3
  83.2 0.8 copy-start.5
  84.0 38.0 %all-to-all-start.1 = ((bf16[16,8,2048]{2,1,0:T(8,128)(2,1)}), bf16[16,8,2048]{2,1,0:T(8,128)(2,1)S(1)}, u32[]{:S(2)}, u32[]{:S(2)}) async-start(bf16[16,8,2048]{2,1,0:T(8,128)(2,1)} %bitcast.66), calls=%async_computation.1 | async-start | bytes 1048576 | tf_op jit(solution)/shard_map/all_to_all | solution.py:165
  94.5 21.7 %collective-permute-start.8 = (bf16[2,384,256]{2,1,0:T(8,128)(2,1)S(1)}, bf16[2,384,256]{2,1,0:T(8,128)(2,1)S(1)}, u32[]{:S(2)}, u32[]{:S(2)}) collective-permute-start(bf16[2,384,256]{2,1,0:T(8,128)(2,1)S(1)} %get-tuple-element.25), channel_id=1, source_target_pairs={{0,6},{2,4},{4,2},{6,0},{1,7},{3,5},{5,3},{7,1},{8,14},{10,12},{12... | collective-permute-start | bytes 1179656 | tf_op jit(solution)/shard_map/ppermute | solution.py:150
  96.4 19.8 %collective-permute-start.7 = (bf16[2,384,256]{2,1,0:T(8,128)(2,1)S(1)}, bf16[2,384,256]{2,1,0:T(8,128)(2,1)S(1)}, u32[]{:S(2)}, u32[]{:S(2)}) collective-permute-start(bf16[2,384,256]{2,1,0:T(8,128)(2,1)S(1)} %get-tuple-element.25), channel_id=1, source_target_pairs={{0,4},{2,6},{4,0},{6,2},{1,5},{3,7},{5,1},{7,3},{8,12},{10,14},{12... | collective-permute-start | bytes 1179656 | tf_op jit(solution)/shard_map/ppermute | solution.py:150
  98.3 20.5 %collective-permute-start.6 = (bf16[2,384,256]{2,1,0:T(8,128)(2,1)S(1)}, bf16[2,384,256]{2,1,0:T(8,128)(2,1)}, u32[]{:S(2)}, u32[]{:S(2)}) collective-permute-start(bf16[2,384,256]{2,1,0:T(8,128)(2,1)S(1)} %get-tuple-element.25), channel_id=1, source_target_pairs={{0,2},{2,0},{4,6},{6,4},{1,3},{3,1},{5,7},{7,5},{8,10},{10,8},{12,... | collective-permute-start | bytes 1179656 | tf_op jit(solution)/shard_map/ppermute | solution.py:150
  120.0 14.7 %collective-permute-start.9 = (bf16[4,2,384,256]{3,2,1,0:T(8,128)(2,1)S(1)}, bf16[4,2,384,256]{3,2,1,0:T(8,128)(2,1)}, u32[]{:S(2)}, u32[]{:S(2)}) collective-permute-start(bf16[4,2,384,256]{3,2,1,0:T(8,128)(2,1)S(1)} %pad_maximum_fusion.own), channel_id=1, source_target_pairs={{0,1},{1,0},{2,3},{3,2},{4,5},{5,4},{6,7},{7,6},{8,9},{9,8},{10,11... | collective-permute-start | bytes 4718600 | tf_op jit(solution)/shard_map/ppermute | solution.py:152
  124.8 28.0 %all-to-all-start.2 = ((bf16[16,8,2048]{2,1,0:T(8,128)(2,1)}), bf16[16,8,2048]{2,1,0:T(8,128)(2,1)S(1)}, u32[]{:S(2)}, u32[]{:S(2)}) async-start(bf16[16,8,2048]{2,1,0:T(8,128)(2,1)} %broadcast_in_dim.12), calls=%async_computation.2 | async-start | bytes 1048576 | tf_op jit(solution)/shard_map/all_to_all | solution.py:62
  155.2 23.3 %copy-start.7 = (bf16[2048,128]{1,0:T(8,128)(2,1)}, bf16[2048,128]{1,0:T(8,128)(2,1)S(1)}, u32[]{:S(2)}) copy-start(bf16[2048,128]{1,0:T(8,128)(2,1)S(1)} %get-tuple-element.18) | copy-start | bytes 1572868
  179.3 6.9 %copy-start.6 = (bf16[2048,128]{1,0:T(8,128)(2,1)S(1)}, bf16[2048,128]{1,0:T(8,128)(2,1)}, u32[]{:S(2)}) copy-start(bf16[2048,128]{1,0:T(8,128)(2,1)} %copy-done.5) | copy-start | bytes 1572868
  179.4 6.9 %copy-start.8 = (bf16[2048,128]{1,0:T(8,128)(2,1)S(1)}, bf16[2048,128]{1,0:T(8,128)(2,1)}, u32[]{:S(2)}) copy-start(bf16[2048,128]{1,0:T(8,128)(2,1)} %copy-done.7) | copy-start | bytes 1572868
  180.5 34.0 %all-to-all-start.4 = ((bf16[32,8,2048]{2,1,0:T(8,128)(2,1)}), bf16[32,8,2048]{2,1,0:T(8,128)(2,1)S(1)}, u32[]{:S(2)}, u32[]{:S(2)}) async-start(bf16[32,8,2048]{2,1,0:T(8,128)(2,1)} %broadcast_in_dim.28), calls=%async_computation.4 | async-start | bytes 2097152 | tf_op jit(solution)/shard_map/all_to_all | solution.py:62
  186.2 1.1 copy-start.4
  187.3 1.2 copy-start.2
where the time goes:
time: 217 us; the launch traced here: 215 us
  starting transfers between devices  87 us (40%)
  waiting for transfers between devices  82.5 us (38%)
  blocking collectives  23.2 us (11%)
  other arithmetic  9.51 us (4%)
  local copies, waits for them, and re-layouts  8.63 us (4%)
  Pallas kernels  3.57 us (2%)
    all_to_all x3, waiting for transfers between devices, to_everyone(): lax.all_to_all(jnp.broadcast_to(value[None], (count, *value.shape)), axes...  43 us
    all_to_all x1, blocking collectives, step(): lax.all_to_all(part.reshape(16, 8, 2048), ('zl', 'yh'), 0, 0, tiled=True)  23.2 us
    all_to_all x3, starting transfers between devices, to_everyone(): lax.all_to_all(jnp.broadcast_to(value[None], (count, *value.shape)), axes...  22.5 us
    ppermute x2, waiting for transfers between devices, step(): moved.append(lax.ppermute(block, AXES, weight_moves()))  18.6 us
    ppermute x3, waiting for transfers between devices, step(): lax.ppermute(pair, 'x', [(x, x ^ k) for x in range(4)])  14.5 us
    ppermute x1, starting transfers between devices, step(): across = lax.ppermute(both, 'gr', SWAP)  13.3 us
    ppermute x2, starting transfers between devices, step(): moved.append(lax.ppermute(block, AXES, weight_moves()))  12.3 us
    all_to_all x1, starting transfers between devices, step(): lax.all_to_all(part.reshape(16, 8, 2048), ('zl', 'yh'), 0, 0, tiled=True)  10.4 us
  transfers between devices with their start and end apart: 14, of which 8 were waited for; matrix products, arithmetic and copies ran while one was open for 4% of the time, Pallas kernels for 1%

commit v1 on v0

--- a/solution.py
+++ b/solution.py
@@ -120,6 +120,31 @@
     return kernel(body, (stream.shape,))(stream)[0]
 
 
+def fold_call(last, parts, mine):
+    count = 32 if last else 16
+
+    def body(parts, mine, sends, total):
+        value = mine[...]
+        summed = parts[0].astype(f32)
+        for i in range(1, 16):
+            summed = summed + parts[i].astype(f32)
+        value = value + 0.5 * summed
+        total[...] = value
+        sent = value.astype(bf16) if last else normalised(value)
+        for i in range(count):
+            sends[i] = sent
+
+    here = pl.BlockSpec(memory_space=pltpu.VMEM)
+    return pl.pallas_call(
+        body,
+        in_specs=[here, here],
+        out_specs=(here, here),
+        out_shape=(pltpu.VMEM((count, 8, 2048), bf16), pltpu.VMEM((8, 2048), f32)),
+        compiler_params=pltpu.CompilerParams(vmem_limit_bytes=24 << 20),
+        name="fold",
+    )(in_vmem(parts), in_vmem(mine))
+
+
 def step(prompt, norm_gain, gate_weight, up_weight, down_weight):
     gain = norm_gain[:, :, None]
     gate = (gain * gate_weight).astype(bf16)
@@ -130,18 +155,24 @@
         block = jnp.concatenate([gate[layer], up[layer]], axis=0)
         moved.append(lax.ppermute(block, AXES, weight_moves()))
     down = down_weight.astype(bf16)
-    both = jnp.concatenate([moved[0], jnp.concatenate([down[0], down[1]], axis=1)], axis=0)
+
+    def with_down(layer):
+        packed = jnp.concatenate([down[layer, :64], down[layer, 64:]], axis=1)
+        return jnp.concatenate([moved[layer], packed], axis=0)
+
+    def unpacked(low, top):
+        upper = jnp.concatenate([low[128:, :128], top[128:, :128]], axis=1)
+        lower = jnp.concatenate([low[128:, 128:], top[128:, 128:]], axis=1)
+        return jnp.concatenate([low[:128], top[:128], upper, lower], axis=0)
+
+    both = with_down(0)
     across = lax.ppermute(both, "gr", SWAP)
-    low, top = in_order(both, across, high)
-
-    def downs(layer):
-        cols = slice(128 * layer, 128 * layer + 128)
-        return jnp.concatenate([low[128:, cols], top[128:, cols]], axis=1)
-
-    block = jnp.concatenate([low[:128], top[:128], downs(0)], axis=0)
+    block = unpacked(*in_order(both, across, high))
+
     own = to_everyone(block, ("x", "yl"), 8)
-    across = lax.ppermute(moved[1], "gr", SWAP)
-    block = jnp.concatenate([*in_order(moved[1], across, high), downs(1)], axis=0)
+    both = with_down(1)
+    across = lax.ppermute(both, "gr", SWAP)
+    block = unpacked(*in_order(both, across, high))
     yl = lax.axis_index("yl")
     came = lax.ppermute(block, "yl", SWAP)
     own, block = lax.optimization_barrier((own, block))
@@ -163,12 +194,11 @@
         ups.append(up)
         served.append(down)
         parts = lax.all_to_all(part.reshape(16, 8, 2048), ("zl", "yh"), 0, 0, tiled=True)
-        mine = mine + 0.5 * jnp.sum(parts.astype(f32), axis=0)
-        if layer == 0:
-            normed = to_everyone(normalised(mine), ("zl", "yh"), 16).reshape(128, 2048)
-        else:
-            mixed = to_everyone(mine.astype(bf16), ("yl", "zl", "yh"), 32)
-    return jnp.stack(gates), jnp.stack(ups), jnp.stack(served), mixed.reshape(prompt.shape)
+        sends, mine = fold_call(layer == 1, parts, mine)
+        axes = ("yl", "zl", "yh") if layer else ("zl", "yh")
+        normed = lax.all_to_all(sends, axes, 0, 0, tiled=True).reshape(-1, 2048)
+    stacks = jnp.stack(gates), jnp.stack(ups), jnp.stack(served)
+    return *stacks, normed.reshape(prompt.shape)
 
 
 def solution(mesh):

time: 217 us -> 211 us (0.972)
  the two profiles are of different devices: /device:TPU:22 before, /device:TPU:16 now
where the time goes in v1:
time: 211 us; the launch traced here: 210 us
  starting transfers between devices  87.8 us (42%)
  waiting for transfers between devices  78.7 us (37%)
  blocking collectives  22.8 us (11%)
  other arithmetic  8.43 us (4%)
  Pallas kernels  5.7 us (3%)
  local copies, waits for them, and re-layouts  5.66 us (3%)
    all_to_all x2, waiting for transfers between devices, step(): normed = lax.all_to_all(sends, axes, 0, 0, tiled=True).reshape(-1, 2048)  41.4 us
    ppermute x2, starting transfers between devices, step(): across = lax.ppermute(both, 'gr', SWAP)  24.3 us
    all_to_all x1, blocking collectives, step(): lax.all_to_all(part.reshape(16, 8, 2048), ('zl', 'yh'), 0, 0, tiled=True)  22.8 us
    ppermute x2, waiting for transfers between devices, step(): moved.append(lax.ppermute(block, AXES, weight_moves()))  14.4 us
    ppermute x3, starting transfers between devices, step(): lax.ppermute(pair, 'x', [(x, x ^ k) for x in range(4)])  13.5 us
    all_to_all x1, waiting for transfers between devices, step(): lax.all_to_all(part.reshape(16, 8, 2048), ('zl', 'yh'), 0, 0, tiled=True)  12.2 us
    all_to_all x1, starting transfers between devices, step(): lax.all_to_all(part.reshape(16, 8, 2048), ('zl', 'yh'), 0, 0, tiled=True)  11.4 us
    all_to_all x2, starting transfers between devices, step(): normed = lax.all_to_all(sends, axes, 0, 0, tiled=True).reshape(-1, 2048)  11 us
  transfers between devices with their start and end apart: 14, of which 8 were waited for; matrix products, arithmetic and copies ran while one was open for 4% of the time, Pallas kernels for 1%

profile of v1, /device:TPU:16, one launch (start us, length us, event | category | flops | bytes accessed | tf_op | source)
XLA Modules:
  0.0 210.2 jit_solution(18216940499344029793)
XLA Ops:
  0.6 1.1 multiply_convert_fusion.1
  1.7 1.9 collective-permute-start
  4.6 3.7 %collective-permute-done = bf16[128,256]{1,0:T(8,128)(2,1)S(1)} collective-permute-done((bf16[128,256]{1,0:T(8,128)(2,1)S(1)}, bf16[128,256]{1,0:T(8,128)(2,1)S(1)}, u32[]{:S(2)}, u32[]{:S(2)}) %collective-permute-start) | collective-permute-done | bytes 65568 | tf_op jit(solution)/shard_map/ppermute | solution.py:156
  8.3 13.9 %collective-permute-start.1 = (bf16[192,256]{1,0:T(8,128)(2,1)S(1)}, bf16[192,256]{1,0:T(8,128)(2,1)S(1)}, u32[]{:S(2)}, u32[]{:S(2)}) collective-permute-start(bf16[192,256]{1,0:T(8,128)(2,1)S(1)} %maximum_maximum_fusion.2), channel_id=1, source_target_pairs={{0,256},{256,0},{1,257},{257,1},{2,258},{258,2},{3,259},{259,3},{4... | collective-permute-start | bytes 294920 | tf_op jit(solution)/shard_map/ppermute | solution.py:169
  22.2 2.6 %collective-permute-done.1 = bf16[192,256]{1,0:T(8,128)(2,1)S(1)} collective-permute-done((bf16[192,256]{1,0:T(8,128)(2,1)S(1)}, bf16[192,256]{1,0:T(8,128)(2,1)S(1)}, u32[]{:S(2)}, u32[]{:S(2)}) %collective-permute-start.1) | collective-permute-done | bytes 98336 | tf_op jit(solution)/shard_map/ppermute | solution.py:169
  25.0 1.3 broadcast_in_dim.2
  26.2 9.8 %all-to-all-start = ((bf16[8,384,256]{2,1,0:T(8,128)(2,1)}), bf16[8,384,256]{2,1,0:T(8,128)(2,1)S(1)}, u32[]{:S(2)}, u32[]{:S(2)}) async-start(bf16[8,384,256]{2,1,0:T(8,128)(2,1)} %broadcast_in_dim.2), calls=%async_computation | async-start | bytes 3145728 | tf_op jit(solution)/shard_map/all_to_all | solution.py:62
  36.1 1.9 collective-permute-start.2
  38.0 10.7 %collective-permute-done.2 = bf16[128,256]{1,0:T(8,128)(2,1)S(1)} collective-permute-done((bf16[128,256]{1,0:T(8,128)(2,1)S(1)}, bf16[128,256]{1,0:T(8,128)(2,1)S(1)}, u32[]{:S(2)}, u32[]{:S(2)}) %collective-permute-start.2) | collective-permute-done | bytes 65568 | tf_op jit(solution)/shard_map/ppermute | solution.py:156
  48.7 10.4 %collective-permute-start.3 = (bf16[192,256]{1,0:T(8,128)(2,1)S(1)}, bf16[192,256]{1,0:T(8,128)(2,1)S(1)}, u32[]{:S(2)}, u32[]{:S(2)}) collective-permute-start(bf16[192,256]{1,0:T(8,128)(2,1)S(1)} %maximum_maximum_fusion.3), channel_id=1, source_target_pairs={{0,256},{256,0},{1,257},{257,1},{2,258},{258,2},{3,259},{259,3},{4... | collective-permute-start | bytes 294920 | tf_op jit(solution)/shard_map/ppermute | solution.py:174
  59.1 2.6 %collective-permute-done.3 = bf16[192,256]{1,0:T(8,128)(2,1)S(1)} collective-permute-done((bf16[192,256]{1,0:T(8,128)(2,1)S(1)}, bf16[192,256]{1,0:T(8,128)(2,1)S(1)}, u32[]{:S(2)}, u32[]{:S(2)}) %collective-permute-start.3) | collective-permute-done | bytes 98336 | tf_op jit(solution)/shard_map/ppermute | solution.py:174
  61.9 1.9 collective-permute-start.4
  63.8 10.1 %collective-permute-start.5 = (bf16[384,256]{1,0:T(8,128)(2,1)S(1)}, bf16[384,256]{1,0:T(8,128)(2,1)S(1)}, u32[]{:S(2)}, u32[]{:S(2)}) collective-permute-start(bf16[384,256]{1,0:T(8,128)(2,1)S(1)} %maximum_maximum_fusion.1), channel_id=1, source_target_pairs={{0,8},{8,0},{1,9},{9,1},{2,10},{10,2},{3,11},{11,3},{4,12},{12,4},... | collective-permute-start | bytes 589832 | tf_op jit(solution)/shard_map/ppermute | solution.py:177
  73.9 5.5 %collective-permute-done.5 = bf16[384,256]{1,0:T(8,128)(2,1)S(1)} collective-permute-done((bf16[384,256]{1,0:T(8,128)(2,1)S(1)}, bf16[384,256]{1,0:T(8,128)(2,1)S(1)}, u32[]{:S(2)}, u32[]{:S(2)}) %collective-permute-start.5) | collective-permute-done | bytes 196640 | tf_op jit(solution)/shard_map/ppermute | solution.py:177
  80.3 8.8 %collective-permute-start.8 = (bf16[2,384,256]{2,1,0:T(8,128)(2,1)}, bf16[2,384,256]{2,1,0:T(8,128)(2,1)}, u32[]{:S(2)}, u32[]{:S(2)}) collective-permute-start(bf16[2,384,256]{2,1,0:T(8,128)(2,1)} %get-tuple-element.31), channel_id=1, source_target_pairs={{0,6},{2,4},{4,2},{6,0},{1,7},{3,5},{5,3},{7,1},{8,14},{10,12},{12... | collective-permute-start | bytes 1179656 | tf_op jit(solution)/shard_map/ppermute | solution.py:181
  89.1 2.4 %collective-permute-start.7 = (bf16[2,384,256]{2,1,0:T(8,128)(2,1)}, bf16[2,384,256]{2,1,0:T(8,128)(2,1)}, u32[]{:S(2)}, u32[]{:S(2)}) collective-permute-start(bf16[2,384,256]{2,1,0:T(8,128)(2,1)} %get-tuple-element.31), channel_id=1, source_target_pairs={{0,4},{2,6},{4,0},{6,2},{1,5},{3,7},{5,1},{7,3},{8,12},{10,14},{12... | collective-permute-start | bytes 1179656 | tf_op jit(solution)/shard_map/ppermute | solution.py:181
  91.5 2.3 %collective-permute-start.6 = (bf16[2,384,256]{2,1,0:T(8,128)(2,1)}, bf16[2,384,256]{2,1,0:T(8,128)(2,1)}, u32[]{:S(2)}, u32[]{:S(2)}) collective-permute-start(bf16[2,384,256]{2,1,0:T(8,128)(2,1)} %get-tuple-element.31), channel_id=1, source_target_pairs={{0,2},{2,0},{4,6},{6,4},{1,3},{3,1},{5,7},{7,5},{8,10},{10,8},{12,... | collective-permute-start | bytes 1179656 | tf_op jit(solution)/shard_map/ppermute | solution.py:181
  98.3 11.4 %all-to-all-start.1 = ((bf16[16,8,2048]{2,1,0:T(8,128)(2,1)}), bf16[16,8,2048]{2,1,0:T(8,128)(2,1)S(1)}, u32[]{:S(2)}, u32[]{:S(2)}) async-start(bf16[16,8,2048]{2,1,0:T(8,128)(2,1)} %bitcast.45), calls=%async_computation.1 | async-start | bytes 1048576 | tf_op jit(solution)/shard_map/all_to_all | solution.py:196
  109.7 1.4 pad_maximum_fusion.own
  111.1 1.9 collective-permute-start.9
  113.9 12.2 %all-to-all-done.1.parts = bf16[16,8,2048]{2,1,0:T(8,128)(2,1)S(1)} async-done(((bf16[16,8,2048]{2,1,0:T(8,128)(2,1)}), bf16[16,8,2048]{2,1,0:T(8,128)(2,1)S(1)}, u32[]{:S(2)}, u32[]{:S(2)}) %all-to-all-start.1) | async-done | bytes 524320 | tf_op jit(solution)/shard_map/all_to_all | solution.py:196
  126.2 1.0 fold.2
  127.2 5.3 %all-to-all-start.2 = ((bf16[16,8,2048]{2,1,0:T(8,128)(2,1)}), bf16[16,8,2048]{2,1,0:T(8,128)(2,1)S(1)}, u32[]{:S(2)}, u32[]{:S(2)}) async-start(bf16[16,8,2048]{2,1,0:T(8,128)(2,1)} %get-tuple-element.20), calls=%async_computation.2 | async-start | bytes 1048576 | tf_op jit(solution)/shard_map/all_to_all | solution.py:199
  132.5 16.4 %all-to-all-done.2 = bf16[16,8,2048]{2,1,0:T(8,128)(2,1)S(1)} async-done(((bf16[16,8,2048]{2,1,0:T(8,128)(2,1)}), bf16[16,8,2048]{2,1,0:T(8,128)(2,1)S(1)}, u32[]{:S(2)}, u32[]{:S(2)}) %all-to-all-start.2) | async-done | bytes 524320 | tf_op jit(solution)/shard_map/all_to_all | solution.py:199
  148.9 2.4 %shard_map.86 = (bf16[2048,128]{1,0:T(8,128)(2,1)S(1)}, bf16[2048,128]{1,0:T(8,128)(2,1)S(1)}, bf16[128,2048]{1,0:T(8,128)(2,1)S(1)}, bf16[128,2048]{1,0:T(8,128)(2,1)S(1)}) custom-call(bf16[128,2048]{1,0:T(8,128)(2,1)S(1)} %bitcast.43, bf16[4,2,384,256]{3,2,1,0:T(8,128)(2,1)S(1)} %pad_maximum_fusion.own, bf16[4,2,384,256]{3,2,1,0:T(8,128)(2,1)} %collective-permute-done.9.other), custom_call_target="tpu_custom_call" | custom-call | tf_op jit(solution)/shard_map/pallas_call | solution.py:45
  151.3 22.8 %all_to_all.25.parts = bf16[16,8,2048]{2,1,0:T(8,128)(2,1)S(1)} all-to-all(bf16[16,8,2048]{2,1,0:T(8,128)(2,1)S(1)} %bitcast.46), channel_id=1, replica_groups=mesh['gr'=2,'zl'=4,'yh'=4,'yl'=2,'x'=4,'core'=2] {'zl','yh'}, dimensions={0} | all-to-all | bytes 1048576 | tf_op jit(solution)/shard_map/all_to_all | solution.py:196
  174.2 1.1 fold.3
  175.3 5.7 %all-to-all-start.4 = ((bf16[32,8,2048]{2,1,0:T(8,128)(2,1)}), bf16[32,8,2048]{2,1,0:T(8,128)(2,1)S(1)}, u32[]{:S(2)}, u32[]{:S(2)}) async-start(bf16[32,8,2048]{2,1,0:T(8,128)(2,1)} %get-tuple-element.29), calls=%async_computation.4 | async-start | bytes 2097152 | tf_op jit(solution)/shard_map/all_to_all | solution.py:199
  181.0 1.1 pad_maximum_fusion.1
  182.1 1.1 pad_maximum_fusion.2
  183.3 1.1 pad_maximum_fusion.3
  184.3 24.9 %all-to-all-done.4 = bf16[32,8,2048]{2,1,0:T(8,128)(2,1)S(1)} async-done(((bf16[32,8,2048]{2,1,0:T(8,128)(2,1)}), bf16[32,8,2048]{2,1,0:T(8,128)(2,1)S(1)}, u32[]{:S(2)}, u32[]{:S(2)}) %all-to-all-start.4) | async-done | bytes 1048608 | tf_op jit(solution)/shard_map/all_to_all | solution.py:199
  (52 shorter events, 8.3 us)
Async XLA Ops:
  1.7 6.5 %collective-permute-start = (bf16[128,256]{1,0:T(8,128)(2,1)S(1)}, bf16[128,256]{1,0:T(8,128)(2,1)S(1)}, u32[]{:S(2)}, u32[]{:S(2)}) collective-permute-start(bf16[128,256]{1,0:T(8,128)(2,1)S(1)} %pad_maximum_fusion.5), channel_id=1, source_target_pairs={{0,0},{1,16},{2,32},{3,48},{4,64},{5,80},{6,96},{7,112},{8,8},{9,2... | collective-permute-start | bytes 196616 | tf_op jit(solution)/shard_map/ppermute | solution.py:156
  8.3 16.5 %collective-permute-start.1 = (bf16[192,256]{1,0:T(8,128)(2,1)S(1)}, bf16[192,256]{1,0:T(8,128)(2,1)S(1)}, u32[]{:S(2)}, u32[]{:S(2)}) collective-permute-start(bf16[192,256]{1,0:T(8,128)(2,1)S(1)} %maximum_maximum_fusion.2), channel_id=1, source_target_pairs={{0,256},{256,0},{1,257},{257,1},{2,258},{258,2},{3,259},{259,3},{4... | collective-permute-start | bytes 294920 | tf_op jit(solution)/shard_map/ppermute | solution.py:169
  26.2 35.6 %all-to-all-start = ((bf16[8,384,256]{2,1,0:T(8,128)(2,1)}), bf16[8,384,256]{2,1,0:T(8,128)(2,1)S(1)}, u32[]{:S(2)}, u32[]{:S(2)}) async-start(bf16[8,384,256]{2,1,0:T(8,128)(2,1)} %broadcast_in_dim.2), calls=%async_computation | async-start | bytes 3145728 | tf_op jit(solution)/shard_map/all_to_all | solution.py:62
  36.1 12.6 %collective-permute-start.2 = (bf16[128,256]{1,0:T(8,128)(2,1)S(1)}, bf16[128,256]{1,0:T(8,128)(2,1)S(1)}, u32[]{:S(2)}, u32[]{:S(2)}) collective-permute-start(bf16[128,256]{1,0:T(8,128)(2,1)S(1)} %pad_maximum_fusion.6), channel_id=1, source_target_pairs={{0,0},{1,16},{2,32},{3,48},{4,64},{5,80},{6,96},{7,112},{8,8},{9,2... | collective-permute-start | bytes 196616 | tf_op jit(solution)/shard_map/ppermute | solution.py:156
  48.7 13.0 %collective-permute-start.3 = (bf16[192,256]{1,0:T(8,128)(2,1)S(1)}, bf16[192,256]{1,0:T(8,128)(2,1)S(1)}, u32[]{:S(2)}, u32[]{:S(2)}) collective-permute-start(bf16[192,256]{1,0:T(8,128)(2,1)S(1)} %maximum_maximum_fusion.3), channel_id=1, source_target_pairs={{0,256},{256,0},{1,257},{257,1},{2,258},{258,2},{3,259},{259,3},{4... | collective-permute-start | bytes 294920 | tf_op jit(solution)/shard_map/ppermute | solution.py:174
  61.9 32.2 %collective-permute-start.4 = (bf16[8,384,256]{2,1,0:T(8,128)(2,1)S(1)}, bf16[8,384,256]{2,1,0:T(8,128)(2,1)S(1)}, u32[]{:S(2)}, u32[]{:S(2)}) collective-permute-start(bf16[8,384,256]{2,1,0:T(8,128)(2,1)S(1)} %all-to-all-done), channel_id=1, source_target_pairs={{0,1},{1,0},{2,3},{3,2},{4,5},{5,4},{6,7},{7,6},{8,9},{9,8},{10,11... | collective-permute-start | bytes 4718600 | tf_op jit(solution)/shard_map/ppermute | solution.py:179
  63.8 15.7 %collective-permute-start.5 = (bf16[384,256]{1,0:T(8,128)(2,1)S(1)}, bf16[384,256]{1,0:T(8,128)(2,1)S(1)}, u32[]{:S(2)}, u32[]{:S(2)}) collective-permute-start(bf16[384,256]{1,0:T(8,128)(2,1)S(1)} %maximum_maximum_fusion.1), channel_id=1, source_target_pairs={{0,8},{8,0},{1,9},{9,1},{2,10},{10,2},{3,11},{11,3},{4,12},{12,4},... | collective-permute-start | bytes 589832 | tf_op jit(solution)/shard_map/ppermute | solution.py:177
  73.9 19.9 %copy-start.9 = (bf16[1,256,2048]{2,1,0:T(8,128)(2,1)S(1)}, bf16[1,256,2048]{2,1,0:T(8,128)(2,1)}, u32[]{:S(2)}) copy-start(bf16[1,256,2048]{2,1,0:T(8,128)(2,1)} %param.5) | copy-start | bytes 3145732
  80.3 29.4 %collective-permute-start.8 = (bf16[2,384,256]{2,1,0:T(8,128)(2,1)}, bf16[2,384,256]{2,1,0:T(8,128)(2,1)}, u32[]{:S(2)}, u32[]{:S(2)}) collective-permute-start(bf16[2,384,256]{2,1,0:T(8,128)(2,1)} %get-tuple-element.31), channel_id=1, source_target_pairs={{0,6},{2,4},{4,2},{6,0},{1,7},{3,5},{5,3},{7,1},{8,14},{10,12},{12... | collective-permute-start | bytes 1179656 | tf_op jit(solution)/shard_map/ppermute | solution.py:181
  89.1 20.6 %collective-permute-start.7 = (bf16[2,384,256]{2,1,0:T(8,128)(2,1)}, bf16[2,384,256]{2,1,0:T(8,128)(2,1)}, u32[]{:S(2)}, u32[]{:S(2)}) collective-permute-start(bf16[2,384,256]{2,1,0:T(8,128)(2,1)} %get-tuple-element.31), channel_id=1, source_target_pairs={{0,4},{2,6},{4,0},{6,2},{1,5},{3,7},{5,1},{7,3},{8,12},{10,14},{12... | collective-permute-start | bytes 1179656 | tf_op jit(solution)/shard_map/ppermute | solution.py:181
  91.5 18.2 %collective-permute-start.6 = (bf16[2,384,256]{2,1,0:T(8,128)(2,1)}, bf16[2,384,256]{2,1,0:T(8,128)(2,1)}, u32[]{:S(2)}, u32[]{:S(2)}) collective-permute-start(bf16[2,384,256]{2,1,0:T(8,128)(2,1)} %get-tuple-element.31), channel_id=1, source_target_pairs={{0,2},{2,0},{4,6},{6,4},{1,3},{3,1},{5,7},{7,5},{8,10},{10,8},{12,... | collective-permute-start | bytes 1179656 | tf_op jit(solution)/shard_map/ppermute | solution.py:181
  95.1 0.8 copy-start
  95.9 0.8 copy-start.1
  96.7 0.8 copy-start.3
  97.5 0.8 copy-start.5
  98.3 27.9 %all-to-all-start.1 = ((bf16[16,8,2048]{2,1,0:T(8,128)(2,1)}), bf16[16,8,2048]{2,1,0:T(8,128)(2,1)S(1)}, u32[]{:S(2)}, u32[]{:S(2)}) async-start(bf16[16,8,2048]{2,1,0:T(8,128)(2,1)} %bitcast.45), calls=%async_computation.1 | async-start | bytes 1048576 | tf_op jit(solution)/shard_map/all_to_all | solution.py:196
  111.1 21.3 %collective-permute-start.9 = (bf16[4,2,384,256]{3,2,1,0:T(8,128)(2,1)S(1)}, bf16[4,2,384,256]{3,2,1,0:T(8,128)(2,1)}, u32[]{:S(2)}, u32[]{:S(2)}) collective-permute-start(bf16[4,2,384,256]{3,2,1,0:T(8,128)(2,1)S(1)} %pad_maximum_fusion.own), channel_id=1, source_target_pairs={{0,1},{1,0},{2,3},{3,2},{4,5},{5,4},{6,7},{7,6},{8,9},{9,8},{10,11... | collective-permute-start | bytes 4718600 | tf_op jit(solution)/shard_map/ppermute | solution.py:183
  127.2 21.7 %all-to-all-start.2 = ((bf16[16,8,2048]{2,1,0:T(8,128)(2,1)}), bf16[16,8,2048]{2,1,0:T(8,128)(2,1)S(1)}, u32[]{:S(2)}, u32[]{:S(2)}) async-start(bf16[16,8,2048]{2,1,0:T(8,128)(2,1)} %get-tuple-element.20), calls=%async_computation.2 | async-start | bytes 1048576 | tf_op jit(solution)/shard_map/all_to_all | solution.py:199
  151.3 22.8 %copy-start.7 = (bf16[2048,128]{1,0:T(8,128)(2,1)}, bf16[2048,128]{1,0:T(8,128)(2,1)S(1)}, u32[]{:S(2)}) copy-start(bf16[2048,128]{1,0:T(8,128)(2,1)S(1)} %get-tuple-element.22) | copy-start | bytes 1572868
  174.1 6.9 %copy-start.6 = (bf16[2048,128]{1,0:T(8,128)(2,1)S(1)}, bf16[2048,128]{1,0:T(8,128)(2,1)}, u32[]{:S(2)}) copy-start(bf16[2048,128]{1,0:T(8,128)(2,1)} %copy-done.5) | copy-start | bytes 1572868
  174.2 6.9 %copy-start.8 = (bf16[2048,128]{1,0:T(8,128)(2,1)S(1)}, bf16[2048,128]{1,0:T(8,128)(2,1)}, u32[]{:S(2)}) copy-start(bf16[2048,128]{1,0:T(8,128)(2,1)} %copy-done.7) | copy-start | bytes 1572868
  175.3 33.9 %all-to-all-start.4 = ((bf16[32,8,2048]{2,1,0:T(8,128)(2,1)}), bf16[32,8,2048]{2,1,0:T(8,128)(2,1)S(1)}, u32[]{:S(2)}, u32[]{:S(2)}) async-start(bf16[32,8,2048]{2,1,0:T(8,128)(2,1)} %get-tuple-element.29), calls=%async_computation.4 | async-start | bytes 2097152 | tf_op jit(solution)/shard_map/all_to_all | solution.py:199
  181.0 1.1 copy-start.4
  182.1 1.2 copy-start.2
